TPU v7x, 512 devices: a 4x2x32 block of a 4x8x32 slice. The times are simulated.
512 devices in a mesh: grp: 2 (over y), ep: 64 (over z, core), tp: 4 (over x).
Axes of the slice: x: 4, y: 2, z: 32, core: 2. Of those that a mesh axis runs over, the one named last changes fastest.
The devices are a block of a 4x8x32 slice.
Arguments:
- tokens: bfloat16 [49152, 2048], P(('grp', 'ep'), 'tp'), parts along dimension 0
- group_choice: int32 [49152], P(('grp', 'ep')), parts along dimension 0, may hold values from 0 to 7, as said below
- expert_choice: int32 [49152, 2], P(('grp', 'ep')), parts along dimension 0, may hold values from 0 to 7, as said below
- group_weight: float32 [49152], P(('grp', 'ep')), parts along dimension 0, may hold values from 0.3 to 1
- expert_weight: float32 [49152, 2], P(('grp', 'ep')), parts along dimension 0, may hold values from 0.1 to 1
- norm_gain: float32 [2048], replicated, may hold values from 0.1 to 1.9
- w_gate: bfloat16 [64, 2048, 1024], P('ep', None, 'tp'), may hold values from -0.125 to 0.125
- w_up: bfloat16 [64, 2048, 1024], P('ep', None, 'tp'), may hold values from -0.125 to 0.125
- w_down: bfloat16 [64, 1024, 2048], P('ep', None, 'tp'), may hold values from -0.1875 to 0.1875
Outputs:
- moe_out: bfloat16 [49152, 2048], P(('grp', 'ep'), 'tp'), parts along dimension 0
There are 2 independent parts, one for each index of `grp`. A program takes and returns all parts, laid end to end along the dimension named above; an argument that names none is the same for every part. Nothing has to cross between parts.
Inputs may be any that keep to these rules, and one draw needn't show every extreme that they name: `group_choice`: group of each token, 0 to 7; within each aligned block of 384 tokens (the tokens of one index of ep) every group is chosen by the same number of tokens. `expert_choice`: a token's two entries differ; within each aligned block of 384 tokens no expert (group with entry) is named by more than 18 tokens, and in every block one expert of each group, the same one in all blocks, is named by exactly 18 tokens.
All inputs are finite; a program needn't handle non-finite values.
Results may differ from a plain program's by a relative error of at most 0.0071.
Values may be sent and summed in bfloat16 or wider, within the bound.
A program may use at most 64 MiB of HBM per device.

v0:
```python
import jax
import jax.numpy as jnp
from jax import lax
from jax.sharding import Mesh
from jax.sharding import PartitionSpec as P

EP = ("ep_0", "ep_1")
GRP_EP = ("grp", "ep_0", "ep_1")


def copy_for_each(array, axis):
    length = lax.axis_size(axis)
    return lax.all_to_all(
        jnp.broadcast_to(array[None], (length, *array.shape)), axis, 0, 0, tiled=True
    )


def laid_out(blocks, dim):
    dims = list(blocks.shape[1:])
    dims[dim] *= blocks.shape[0]
    return jnp.moveaxis(blocks, 0, dim).reshape(dims)


def collect(array, axis, dim):
    blocks = copy_for_each(array, axis)
    return laid_out(blocks, dim)


def over_copies(array, axis):
    everything = copy_for_each(array, axis)
    return jnp.sum(everything, axis=0)


def cut_along(array, dim, length):
    dims = array.shape
    blocks = array.reshape(*dims[:dim], length, dims[dim] // length, *dims[dim + 1 :])
    return jnp.moveaxis(blocks, dim, 0)


def moved_by_axis(blocks, axes, turns):
    dims = [lax.axis_size(a) for a in axes]
    blocks = blocks.reshape(*dims, *blocks.shape[1:])
    for k in turns:
        blocks = lax.all_to_all(blocks, axes[k], split_axis=k, concat_axis=k, tiled=True)
    return blocks.reshape(-1, *blocks.shape[len(axes) :])


def exchange_by_chip(array, groups, turns, split_dim, concat_dim):
    length = lax.axis_size(groups[0]) * lax.axis_size(groups[1])
    blocks = cut_along(array, split_dim, length)
    return laid_out(moved_by_axis(blocks, groups, turns), concat_dim)


def finish_rows(gate_sum, up_sum, w_down):
    hidden = (jax.nn.silu(gate_sum) * up_sum).astype(jnp.bfloat16)
    whole_hidden = collect(hidden, "tp", 3)
    summed = jnp.einsum("sxcf,xfd->sxcd", whole_hidden, w_down, preferred_element_type=jnp.float32)
    return summed.astype(jnp.bfloat16)


def body(
    tokens,
    group_choice,
    expert_choice,
    group_weight,
    expert_weight,
    norm_gain,
    w_gate,
    w_up,
    w_down,
):
    tok_rows = tokens.shape[0]
    ep_count = lax.axis_size(EP)
    exp_local = w_gate.shape[0]
    experts_all = ep_count * exp_local
    group_size = min(8, experts_all // 2)
    group_count = experts_all // group_size
    mean_load = 2 * tok_rows // experts_all
    capacity = mean_load + min(mean_load // 2, tok_rows // group_count - mean_load)
    model_width = norm_gain.shape[0]
    expert_ids = group_choice[:, None] * group_size + expert_choice
    mixing = group_weight[:, None] * expert_weight / jnp.sum(expert_weight, -1, keepdims=True)
    flat_ids = expert_ids.reshape(-1)
    marks = (flat_ids[:, None] == jnp.arange(experts_all, dtype=jnp.int32)[None, :]).astype(
        jnp.int32
    )
    earlier = jnp.cumsum(marks, 0) - marks
    seat_index = jnp.sum(earlier * marks, 1)
    targets = (flat_ids * capacity + seat_index).reshape(tok_rows, 2)
    places = jnp.arange(experts_all * capacity, dtype=jnp.int32)
    dispatch = (
        (places[:, None] == targets[None, :, 0]) | (places[:, None] == targets[None, :, 1])
    ).astype(jnp.bfloat16)
    values = tokens.astype(jnp.float32)
    own_squares = jnp.sum(values * values, -1)
    all_squares = over_copies(own_squares, "tp")
    inv_rms = lax.rsqrt(all_squares / model_width + 1e-06)
    piece_width = tokens.shape[1]
    gain_piece = lax.dynamic_slice_in_dim(
        norm_gain, lax.axis_index("tp") * piece_width, piece_width, 0
    )
    normed = (values * inv_rms[:, None] * gain_piece[None, :]).astype(jnp.bfloat16)
    buffer = jnp.dot(dispatch, normed, preferred_element_type=jnp.float32).astype(jnp.bfloat16)
    buffer = buffer.reshape(ep_count, exp_local, capacity, piece_width)
    piece = lax.all_gather(
        lax.all_to_all(buffer, EP, split_axis=0, concat_axis=0, tiled=True),
        "tp",
        axis=3,
        tiled=True,
    )
    gate_next = jnp.einsum("sxcd,xdf->sxcf", piece, w_gate, preferred_element_type=jnp.float32)
    up_next = jnp.einsum("sxcd,xdf->sxcf", piece, w_up, preferred_element_type=jnp.float32)
    results = finish_rows(gate_next, up_next, w_down)
    returned = exchange_by_chip(results, ("ep_0", "ep_1"), (1, 0), 0, 0)
    returned = returned.reshape(experts_all * capacity, returned.shape[3])
    combined = jnp.zeros((tok_rows, returned.shape[1]), jnp.float32)
    for choice_index in range(2):
        picker = (targets[:, choice_index : choice_index + 1] == places[None, :]).astype(
            jnp.bfloat16
        )
        picked = jnp.dot(picker, returned, preferred_element_type=jnp.float32)
        combined = combined + mixing[:, choice_index : choice_index + 1] * picked
    return combined.astype(jnp.bfloat16)


def solution(mesh):
    split = Mesh(
        mesh.devices.reshape(mesh.shape["grp"], 32, 2, mesh.shape["tp"]),
        ("grp", "ep_0", "ep_1", "tp"),
    )
    placed = (
        P(GRP_EP, "tp"),
        P(GRP_EP),
        P(GRP_EP, None),
        P(GRP_EP),
        P(GRP_EP, None),
        P(),
        P(EP, None, "tp"),
        P(EP, None, "tp"),
        P(EP, None, "tp"),
    )
    return jax.shard_map(
        body, mesh=split, in_specs=placed, out_specs=P(GRP_EP, "tp"), check_vma=False
    )
```

profile of v0, /device:TPU:33, one launch (start us, length us, event | category | flops | bytes accessed | tf_op | source)
XLA Modules:
  0.0 482.4 jit_solution(356377158643691526)
XLA Ops:
  6.6 1.2 fusion.35
  7.8 0.6 broadcast_in_dim.6
  8.4 5.1 %all-to-all-start = ((f32[4,1,384]{2,1,0:T(1,128)}), f32[4,1,384]{2,1,0:T(1,128)S(1)}, u32[]{:S(2)}, u32[]{:S(2)}) async-start(f32[4,1,384]{2,1,0:T(1,128)} %broadcast_in_dim.6), calls=%async_computation | async-start | bytes 12288 | tf_op jit(solution)/shard_map/all_to_all | solution.py:13
  13.5 0.8 copy.35
  14.3 0.7 broadcast_multiply_fusion
  15.5 1.8 reduce-window.6
  17.3 0.3 slice_reduce_fusion.2
  17.7 0.2 reduce_sum.40
  18.0 0.3 slice_reduce_fusion.1
  18.3 0.8 dynamic_slice.3
  19.1 1.9 convolution_convert_fusion
  21.0 2.2 reshape.67
  23.2 199.5 %all_to_all.26 = bf16[64,1,18,512]{3,2,1,0:T(8,128)(2,1)S(1)} all-to-all(bf16[64,1,18,512]{3,2,1,0:T(8,128)(2,1)S(1)} %bitcast.87), channel_id=1, replica_groups=mesh['grp'=2,'ep_0'=32,'ep_1'=2,'tp'=4] {'ep_0','ep_1'}, dimensions={0} | all-to-all | bytes 2359296 | tf_op jit(solution)/shard_map/all_to_all | solution.py:106
  222.7 1.4 copy.39
  224.2 52.9 %all-gather.2.cloned.1.call-done = bf16[64,1,18,2048]{3,0,2,1:T(8,128)(2,1)} async-done(((bf16[64,1,18,512]{3,0,2,1:T(8,128)(2,1)}), bf16[64,1,18,2048]{3,0,2,1:T(8,128)(2,1)}) %all-gather.2.cloned.1.call-update) | async-done | bytes 4718608 | tf_op jit(solution)/shard_map/all_gather | solution.py:105
  277.1 3.9 fusion.9
  281.0 1.5 fusion.25
  282.5 0.3 broadcast_in_dim.8
  282.8 31.1 %all_to_all.27 = bf16[4,64,1,18,256]{4,1,3,2,0:T(8,128)(2,1)S(1)} all-to-all(bf16[4,64,1,18,256]{4,1,3,2,0:T(8,128)(2,1)S(1)} %broadcast_in_dim.8), channel_id=1, replica_groups=mesh['grp'=2,'ep_0'=32,'ep_1'=2,'tp'=4] {'tp'}, dimensions={0} | all-to-all | bytes 4718592 | tf_op jit(solution)/shard_map/all_to_all | solution.py:13
  313.9 2.0 copy.40
  315.9 2.9 reshape.71
  318.8 3.0 fusion.8
  321.9 0.5 reshape_reshape.3
  322.4 0.2 copy.41
  322.6 6.3 %all_to_all.28 = bf16[32,2,1,1,18,512]{5,0,4,3,2,1:T(8,128)(2,1)S(1)} all-to-all(bf16[32,2,1,1,18,512]{5,0,4,3,2,1:T(8,128)(2,1)S(1)} %copy.41), channel_id=1, replica_groups=mesh['grp'=2,'ep_0'=32,'ep_1'=2,'tp'=4] {'ep_1'}, dimensions={1} | all-to-all | bytes 2359296 | tf_op jit(solution)/shard_map/all_to_all | solution.py:44
  328.9 2.3 copy.42
  331.2 23.3 %all-to-all-start.4 = ((bf16[32,2,1,1,18,512]{5,1,4,3,2,0:T(2,128)(2,1)}), bf16[32,2,1,1,18,512]{5,1,4,3,2,0:T(2,128)(2,1)}, u32[]{:S(2)}, u32[]{:S(2)}) async-start(bf16[32,2,1,1,18,512]{5,1,4,3,2,0:T(2,128)(2,1)} %copy.42), calls=%async_computation.4 | async-start | bytes 2359296 | tf_op jit(solution)/shard_map/all_to_all | solution.py:44
  354.6 114.5 %all-to-all-done.4 = bf16[32,2,1,1,18,512]{5,1,4,3,2,0:T(2,128)(2,1)} async-done(((bf16[32,2,1,1,18,512]{5,1,4,3,2,0:T(2,128)(2,1)}), bf16[32,2,1,1,18,512]{5,1,4,3,2,0:T(2,128)(2,1)}, u32[]{:S(2)}, u32[]{:S(2)}) %all-to-all-start.4) | async-done | bytes 1179680 | tf_op jit(solution)/shard_map/all_to_all | solution.py:44
  469.1 1.6 copy.43
  470.7 1.2 reshape_reshape_reshape.3
  472.0 2.1 fusion.23
  474.0 1.5 fusion.24
  (31 shorter events, 0.9 us)
Async XLA Ops:
  6.5 312.3 %copy-start = (bf16[1,1024,512]{2,1,0:T(8,128)(2,1)S(1)}, bf16[1,1024,512]{2,1,0:T(8,128)(2,1)}, u32[]{:S(2)}) copy-start(bf16[1,1024,512]{2,1,0:T(8,128)(2,1)} %param.17) | copy-start | bytes 3145732
  8.4 10.6 %all-to-all-start = ((f32[4,1,384]{2,1,0:T(1,128)}), f32[4,1,384]{2,1,0:T(1,128)S(1)}, u32[]{:S(2)}, u32[]{:S(2)}) async-start(f32[4,1,384]{2,1,0:T(1,128)} %broadcast_in_dim.6), calls=%async_computation | async-start | bytes 12288 | tf_op jit(solution)/shard_map/all_to_all | solution.py:13
  13.5 263.6 %all-gather.2.cloned.1.call-start = ((), (), s32[]{:S(2)}) async-start(), calls=%async_computation.5 | async-start | bytes 5898240 | tf_op jit(solution)/shard_map/all_gather | solution.py:105
  15.3 3.8 copy-start.2
  224.1 53.0 %copy-start.6 = (bf16[1,2048,256]{2,1,0:T(8,128)(2,1)S(1)}, bf16[1,2048,256]{2,1,0:T(8,128)(2,1)}, u32[]{:S(2)}) copy-start(bf16[1,2048,256]{2,1,0:T(8,128)(2,1)} %param.15) | copy-start | bytes 3145732
  224.2 56.8 %copy-start.7 = (bf16[1,2048,256]{2,1,0:T(8,128)(2,1)S(1)}, bf16[1,2048,256]{2,1,0:T(8,128)(2,1)}, u32[]{:S(2)}) copy-start(bf16[1,2048,256]{2,1,0:T(8,128)(2,1)} %param.16) | copy-start | bytes 3145732
  277.1 3.9 copy-start.5
  331.2 23.4 %copy-start.3 = (f32[384,2]{0,1:T(2,128)S(1)}, f32[384,2]{0,1:T(2,128)}, u32[]{:S(2)}) copy-start(f32[384,2]{0,1:T(2,128)} %param.13) | copy-start | bytes 9220
  331.2 23.4 %copy-start.4 = (f32[384]{0:T(512)S(1)}, f32[384]{0:T(512)}, u32[]{:S(2)}) copy-start(f32[384]{0:T(512)} %param.12) | copy-start | bytes 4612
  331.2 137.9 %all-to-all-start.4 = ((bf16[32,2,1,1,18,512]{5,1,4,3,2,0:T(2,128)(2,1)}), bf16[32,2,1,1,18,512]{5,1,4,3,2,0:T(2,128)(2,1)}, u32[]{:S(2)}, u32[]{:S(2)}) async-start(bf16[32,2,1,1,18,512]{5,1,4,3,2,0:T(2,128)(2,1)} %copy.42), calls=%async_computation.4 | async-start | bytes 2359296 | tf_op jit(solution)/shard_map/all_to_all | solution.py:44
  472.0 2.1 copy-start.1
Sparse Core Ops, SparseCore 0:
  224.3 52.7 all-gather.1
where the time goes:
time: 483 us; the launch traced here: 482 us
  blocking collectives  237 us (49%)
  waiting for transfers between devices  167 us (35%)
  starting transfers between devices  28.5 us (6%)
  local copies, waits for them, and re-layouts  17.8 us (4%)
  matrix products  13.9 us (3%)
  between operations  13.6 us (3%)
    all_to_all x1, blocking collectives, body(): lax.all_to_all(buffer, EP, split_axis=0, concat_axis=0, tiled=True)  200 us
    all_to_all x1, waiting for transfers between devices, moved_by_axis(): lax.all_to_all(blocks, axes[k], split_axis=k, concat_axis=k, tiled=True)  115 us
    all_gather x1, waiting for transfers between devices, body(): lax.all_gather(lax.all_to_all(buffer, EP, split_axis=0, concat_axis=0, ti...  52.9 us
    all_to_all x1, blocking collectives, copy_for_each(): lax.all_to_all(jnp.broadcast_to(array[None], (length, *array.shape)), axi...  31.1 us
    all_to_all x1, starting transfers between devices, moved_by_axis(): lax.all_to_all(blocks, axes[k], split_axis=k, concat_axis=k, tiled=True)  23.3 us
  transfers between devices with their start and end apart: 3, of which 2 were waited for; matrix products, arithmetic and copies ran while one was open for 1% of the time, Pallas kernels for 0%

commit v1 on v0

--- a/solution.py
+++ b/solution.py
@@ -3,9 +3,17 @@
 from jax import lax
 from jax.sharding import Mesh
 from jax.sharding import PartitionSpec as P
+from jax.lax import axis_index, axis_size, ppermute
 
 EP = ("ep_0", "ep_1")
 GRP_EP = ("grp", "ep_0", "ep_1")
+
+
+def bring_tables_on_mesh(tile_in, dimension_no):
+    mid_arr = list(tile_in.shape[1:])
+    mid_arr[dimension_no] *= tile_in.shape[0]
+    near = jnp.moveaxis(tile_in, 0, dimension_no).reshape(mid_arr)
+    return near
 
 
 def copy_for_each(array, axis):
@@ -102,11 +110,25 @@
     normed = (values * inv_rms[:, None] * gain_piece[None, :]).astype(jnp.bfloat16)
     buffer = jnp.dot(dispatch, normed, preferred_element_type=jnp.float32).astype(jnp.bfloat16)
     buffer = buffer.reshape(ep_count, exp_local, capacity, piece_width)
-    piece = lax.all_gather(
-        lax.all_to_all(buffer, EP, split_axis=0, concat_axis=0, tiled=True),
-        "tp",
-        axis=3,
-        tiled=True,
+
+    def _recover_cycles(mat, comm_axis, join_dim):
+        axis_len = axis_size(comm_axis)
+        trail = list(map(lambda dev_j: (dev_j, (dev_j + 1) % axis_len), range(axis_len)))
+        copies = [(at, jj) for jj, at in trail]
+        a_now, base_arr = ([], [])
+        for dd in tuple(range(axis_len - 1)):
+            if dd % 2 == 0:
+                a_now.append(ppermute(a_now[-1] if a_now else mat, comm_axis, trail))
+            else:
+                base_arr.append(ppermute(base_arr[-1] if base_arr else mat, comm_axis, copies))
+        g_now = jnp.stack([*a_now[::-1], mat, *base_arr])
+        tile_out = axis_index(comm_axis) - len(a_now)
+        g_now = g_now[(jnp.arange(axis_len) - tile_out) % axis_len]
+        z1 = bring_tables_on_mesh(g_now, join_dim)
+        return z1
+
+    piece = _recover_cycles(
+        lax.all_to_all(buffer, EP, split_axis=0, concat_axis=0, tiled=True), "tp", 3
     )
     gate_next = jnp.einsum("sxcd,xdf->sxcf", piece, w_gate, preferred_element_type=jnp.float32)
     up_next = jnp.einsum("sxcd,xdf->sxcf", piece, w_up, preferred_element_type=jnp.float32)

time: 483 us -> 488 us (1.010)
  local copies, waits for them, and re-layouts: 17.8 us -> 46.9 us
  between operations: 13.6 us -> 0.26 us
  waiting for transfers between devices: 167 us -> 158 us
    all_gather x1 -> x0, waiting for transfers between devices: 52.9 us -> none  [body(): lax.all_gather(lax.all_to_all(buffer, EP, split_axis=0, concat_axis=0, ti...]
    ppermute x0 -> x3, waiting for transfers between devices: none -> 43.8 us  [the longest x2 43.8 us: _recover_cycles(): a_now.append(ppermute(a_now[-1] if a_now else mat, comm_axis, trail))]
    all_to_all x1, starting transfers between devices: 23.3 us -> 9.87 us  [moved_by_axis(): lax.all_to_all(blocks, axes[k], split_axis=k, concat_axis=k, tiled=True)]
    ppermute x0 -> x3, starting transfers between devices: none -> 8.95 us  [the longest x2 5.79 us: _recover_cycles(): a_now.append(ppermute(a_now[-1] if a_now else mat, comm_axis, trail))]
    another operation x1 -> x2, local copies, waits for them, and re-layouts: 2.9 us -> 11.7 us
    transpose x0 -> x1, local copies, waits for them, and re-layouts: none -> 8.64 us  [bring_tables_on_mesh(): near = jnp.moveaxis(tile_in, 0, dimension_no).reshape(mid_arr)]
    gather x0 -> x1, local copies, waits for them, and re-layouts: none -> 6.39 us  [_recover_cycles(): g_now = g_now[(jnp.arange(axis_len) - tile_out) % axis_len]]
    ppermute x0 -> x3, local copies, waits for them, and re-layouts: none -> 5.81 us  [the longest x2 3.88 us: _recover_cycles(): a_now.append(ppermute(a_now[-1] if a_now else mat, comm_axis, trail))]
  transfers between devices with their start and end apart: 3 -> 5, of which waited for: 2 -> 3; matrix products, arithmetic and copies ran while one was open for 1% -> 2% of each run, Pallas kernels for 0% -> 0%
where the time goes in v1:
time: 488 us; the launch traced here: 487 us
  blocking collectives  237 us (49%)
  waiting for transfers between devices  158 us (32%)
  local copies, waits for them, and re-layouts  46.9 us (10%)
  starting transfers between devices  23.9 us (5%)
  matrix products  13 us (3%)
  other arithmetic  8.19 us (2%)
    all_to_all x1, blocking collectives, body(): lax.all_to_all(buffer, EP, split_axis=0, concat_axis=0, tiled=True)  200 us
    all_to_all x1, waiting for transfers between devices, moved_by_axis(): lax.all_to_all(blocks, axes[k], split_axis=k, concat_axis=k, tiled=True)  115 us
    ppermute x2, waiting for transfers between devices, _recover_cycles(): a_now.append(ppermute(a_now[-1] if a_now else mat, comm_axis, trail))  43.8 us
    all_to_all x1, blocking collectives, copy_for_each(): lax.all_to_all(jnp.broadcast_to(array[None], (length, *array.shape)), axi...  27.7 us
    another operation x2, local copies, waits for them, and re-layouts  11.7 us
    all_to_all x1, starting transfers between devices, moved_by_axis(): lax.all_to_all(blocks, axes[k], split_axis=k, concat_axis=k, tiled=True)  9.87 us
  transfers between devices with their start and end apart: 5, of which 3 were waited for; matrix products, arithmetic and copies ran while one was open for 2% of the time, Pallas kernels for 0%

profile of v1, /device:TPU:33, one launch (start us, length us, event | category | flops | bytes accessed | tf_op | source)
XLA Modules:
  0.0 487.2 jit_solution(15552950663809139898)
XLA Ops:
  0.0 1.2 fusion.19
  1.8 5.1 %all-to-all-start = ((f32[4,1,384]{2,1,0:T(1,128)}), f32[4,1,384]{2,1,0:T(1,128)S(1)}, u32[]{:S(2)}, u32[]{:S(2)}) async-start(f32[4,1,384]{2,1,0:T(1,128)} %broadcast_in_dim.6), calls=%async_computation | async-start | bytes 12288 | tf_op jit(solution)/shard_map/all_to_all | solution.py:21
  9.0 1.8 reduce-window.6
  13.5 1.3 reshape.119
  14.8 199.7 %all_to_all.26 = bf16[64,1,18,512]{3,2,1,0:T(8,128)(2,1)S(1)} all-to-all(bf16[64,1,18,512]{3,2,1,0:T(8,128)(2,1)} %bitcast.98), channel_id=1, replica_groups=mesh['grp'=2,'ep_0'=32,'ep_1'=2,'tp'=4] {'ep_0','ep_1'}, dimensions={0} | all-to-all | bytes 2359296 | tf_op jit(solution)/shard_map/all_to_all | solution.py:131
  214.5 1.4 copy.48
  215.9 3.7 collective-permute-start
  219.6 3.2 collective-permute-start.2
  222.8 22.1 %collective-permute-done = bf16[64,1,18,512]{3,0,2,1:T(8,128)(2,1)} collective-permute-done((bf16[64,1,18,512]{3,0,2,1:T(8,128)(2,1)}, bf16[64,1,18,512]{3,0,2,1:T(8,128)(2,1)}, u32[]{:S(2)}, u32[]{:S(2)}) %collective-permute-start) | collective-permute-done | bytes 1179680 | tf_op jit(solution)/shard_map/ppermute | solution.py:121
  244.9 2.1 collective-permute-start.1
  247.0 1.9 copy.65
  249.0 1.9 copy.64
  250.9 21.7 %collective-permute-done.1 = bf16[64,1,18,512]{3,0,2,1:T(8,128)(2,1)} collective-permute-done((bf16[64,1,18,512]{3,0,2,1:T(8,128)(2,1)}, bf16[64,1,18,512]{3,0,2,1:T(8,128)(2,1)}, u32[]{:S(2)}, u32[]{:S(2)}) %collective-permute-start.1) | collective-permute-done | bytes 1179680 | tf_op jit(solution)/shard_map/ppermute | solution.py:121
  272.7 1.9 copy.66
  274.6 4.0 maximum_bitcast_fusion
  278.6 6.4 %gather_fusion = bf16[4,64,18,512]{3,2,1,0:T(8,128)(2,1)} fusion(bf16[4,64,18,512]{3,2,1,0:T(8,128)(2,1)} %maximum_bitcast_fusion, s32[1024]{0:T(1024)S(1)} %pad_clamp_fusion), kind=kCustom, calls=%fused_computation | custom fusion | bytes 9437200 | tf_op jit(solution)/shard_map/gather | solution.py:126
  285.0 8.6 %copy.53 = bf16[64,1,18,4,512]{4,3,0,2,1:T(4,128)(2,1)} copy(bf16[64,1,18,4,512]{4,2,0,3,1:T(8,128)(2,1)} %bitcast.92) | data formatting | bytes 9437184 | tf_op jit(solution)/shard_map/transpose | solution.py:15
  293.6 8.8 %reshape.120 = bf16[64,18,2048]{2,0,1:T(8,128)(2,1)} reshape(bf16[64,1,18,4,512]{4,3,0,2,1:T(4,128)(2,1)} %copy.53) | data formatting | bytes 9437184 | tf_op jit(solution)/shard_map/reshape.4
  302.5 3.9 convolution_bitcast_fusion.1
  306.5 1.5 fusion.11
  308.4 27.7 %all_to_all.27 = bf16[4,64,1,18,256]{4,1,3,2,0:T(8,128)(2,1)S(1)} all-to-all(bf16[4,64,1,18,256]{4,1,3,2,0:T(8,128)(2,1)S(1)} %broadcast_in_dim.8), channel_id=1, replica_groups=mesh['grp'=2,'ep_0'=32,'ep_1'=2,'tp'=4] {'tp'}, dimensions={0} | all-to-all | bytes 4718592 | tf_op jit(solution)/shard_map/all_to_all | solution.py:21
  336.1 2.0 copy.54
  338.2 2.9 reshape.123
  341.1 3.1 fusion.4
  344.9 9.2 %all_to_all.28 = bf16[32,2,1,1,18,512]{5,0,4,3,2,1:T(8,128)(2,1)S(1)} all-to-all(bf16[32,2,1,1,18,512]{5,0,4,3,2,1:T(8,128)(2,1)S(1)} %copy.55), channel_id=1, replica_groups=mesh['grp'=2,'ep_0'=32,'ep_1'=2,'tp'=4] {'ep_1'}, dimensions={1} | all-to-all | bytes 2359296 | tf_op jit(solution)/shard_map/all_to_all | solution.py:52
  354.1 2.3 copy.56
  356.3 9.9 %all-to-all-start.4 = ((bf16[32,2,1,1,18,512]{5,1,4,3,2,0:T(2,128)(2,1)}), bf16[32,2,1,1,18,512]{5,1,4,3,2,0:T(2,128)(2,1)}, u32[]{:S(2)}, u32[]{:S(2)}) async-start(bf16[32,2,1,1,18,512]{5,1,4,3,2,0:T(2,128)(2,1)} %copy.56), calls=%async_computation.4 | async-start | bytes 2359296 | tf_op jit(solution)/shard_map/all_to_all | solution.py:52
  366.3 114.5 %all-to-all-done.4 = bf16[32,2,1,1,18,512]{5,1,4,3,2,0:T(2,128)(2,1)} async-done(((bf16[32,2,1,1,18,512]{5,1,4,3,2,0:T(2,128)(2,1)}), bf16[32,2,1,1,18,512]{5,1,4,3,2,0:T(2,128)(2,1)}, u32[]{:S(2)}, u32[]{:S(2)}) %all-to-all-start.4) | async-done | bytes 1179680 | tf_op jit(solution)/shard_map/all_to_all | solution.py:52
  480.8 1.6 copy.57
  482.4 1.2 reshape_reshape_reshape.3
  483.6 2.1 fusion.9
  485.7 1.5 fusion.10
  (43 shorter events, 6.5 us)
Async XLA Ops:
  0.0 341.1 %copy-start = (bf16[1,1024,512]{2,1,0:T(8,128)(2,1)S(1)}, bf16[1,1024,512]{2,1,0:T(8,128)(2,1)}, u32[]{:S(2)}) copy-start(bf16[1,1024,512]{2,1,0:T(8,128)(2,1)} %param.17) | copy-start | bytes 3145732
  1.8 10.7 %all-to-all-start = ((f32[4,1,384]{2,1,0:T(1,128)}), f32[4,1,384]{2,1,0:T(1,128)S(1)}, u32[]{:S(2)}, u32[]{:S(2)}) async-start(f32[4,1,384]{2,1,0:T(1,128)} %broadcast_in_dim.6), calls=%async_computation | async-start | bytes 12288 | tf_op jit(solution)/shard_map/all_to_all | solution.py:21
  7.0 5.6 %copy-start.3 = (bf16[384,512]{1,0:T(8,128)(2,1)S(1)}, bf16[384,512]{1,0:T(8,128)(2,1)}, u32[]{:S(2)}) copy-start(bf16[384,512]{1,0:T(8,128)(2,1)} %param.9) | copy-start | bytes 1179652
  215.9 28.9 %collective-permute-start = (bf16[64,1,18,512]{3,0,2,1:T(8,128)(2,1)}, bf16[64,1,18,512]{3,0,2,1:T(8,128)(2,1)}, u32[]{:S(2)}, u32[]{:S(2)}) collective-permute-start(bf16[64,1,18,512]{3,0,2,1:T(8,128)(2,1)} %copy.48), channel_id=1, source_target_pairs={{0,1},{1,2},{2,3},{3,0},{4,5},{5,6},{6,7},{7,4},{8,9},{9,10},{10,1... | collective-permute-start | bytes 3538952 | tf_op jit(solution)/shard_map/ppermute | solution.py:121
  219.6 29.4 %collective-permute-start.2 = (bf16[64,1,18,512]{3,0,2,1:T(8,128)(2,1)}, bf16[64,1,18,512]{3,0,2,1:T(8,128)(2,1)}, u32[]{:S(2)}, u32[]{:S(2)}) collective-permute-start(bf16[64,1,18,512]{3,0,2,1:T(8,128)(2,1)} %copy.48), channel_id=1, source_target_pairs={{1,0},{2,1},{3,2},{0,3},{5,4},{6,5},{7,6},{4,7},{9,8},{10,9},{11,1... | collective-permute-start | bytes 3538952 | tf_op jit(solution)/shard_map/ppermute | solution.py:123
  244.9 27.8 %collective-permute-start.1 = (bf16[64,1,18,512]{3,0,2,1:T(8,128)(2,1)}, bf16[64,1,18,512]{3,0,2,1:T(8,128)(2,1)}, u32[]{:S(2)}, u32[]{:S(2)}) collective-permute-start(bf16[64,1,18,512]{3,0,2,1:T(8,128)(2,1)} %collective-permute-done), channel_id=1, source_target_pairs={{0,1},{1,2},{2,3},{3,0},{4,5},{5,6},{6,7},{7,4},{8,9},{9,10},{10,1... | collective-permute-start | bytes 3538952 | tf_op jit(solution)/shard_map/ppermute | solution.py:121
  293.6 8.8 %copy-start.6 = (bf16[1,2048,256]{2,1,0:T(8,128)(2,1)S(1)}, bf16[1,2048,256]{2,1,0:T(8,128)(2,1)}, u32[]{:S(2)}) copy-start(bf16[1,2048,256]{2,1,0:T(8,128)(2,1)} %param.15) | copy-start | bytes 3145732
  302.5 3.9 copy-start.1
  302.5 4.1 copy-start.7
  356.3 9.9 %copy-start.4 = (f32[384,2]{0,1:T(2,128)S(1)}, f32[384,2]{0,1:T(2,128)}, u32[]{:S(2)}) copy-start(f32[384,2]{0,1:T(2,128)} %param.13) | copy-start | bytes 9220
  356.3 9.9 %copy-start.5 = (f32[384]{0:T(512)S(1)}, f32[384]{0:T(512)}, u32[]{:S(2)}) copy-start(f32[384]{0:T(512)} %param.12) | copy-start | bytes 4612
  356.3 124.5 %all-to-all-start.4 = ((bf16[32,2,1,1,18,512]{5,1,4,3,2,0:T(2,128)(2,1)}), bf16[32,2,1,1,18,512]{5,1,4,3,2,0:T(2,128)(2,1)}, u32[]{:S(2)}, u32[]{:S(2)}) async-start(bf16[32,2,1,1,18,512]{5,1,4,3,2,0:T(2,128)(2,1)} %copy.56), calls=%async_computation.4 | async-start | bytes 2359296 | tf_op jit(solution)/shard_map/all_to_all | solution.py:52
  483.6 2.1 copy-start.2
